TPU v7x, 32 devices: a whole 2x2x4 slice. The times are simulated.
32 devices in a mesh: grp: 2 (over y), ra: 4 (over z), cb: 4 (over x, core).
Axes of the slice: x: 2, y: 2, z: 4, core: 2. Of those that a mesh axis runs over, the one named last changes fastest.
Arguments:
- tokens: bfloat16 [512, 4096], P('grp', 'ra'), parts along dimension 0, may hold values from -30 to 30, as said below
- norm_gain: bfloat16 [4096], P('ra'), may hold values from 0.099609375 to 1.8984375
- w_gate: bfloat16 [4096, 11264], P('ra', 'cb'), may hold values from -0.09375 to 0.09375
- w_value: bfloat16 [4096, 11264], P('ra', 'cb'), may hold values from -0.09375 to 0.09375
- conv_gate: float32 [3, 11264], P(None, 'cb'), may hold values from -3 to 3
- conv_value: float32 [3, 11264], P(None, 'cb'), may hold values from -3 to 3
- bias_gate: float32 [11264], P('cb'), may hold values from -3 to 3
- bias_value: float32 [11264], P('cb'), may hold values from -3 to 3
- w_down: bfloat16 [11264, 4096], P('cb', 'ra'), may hold values from -1 to 1
- out_gain: bfloat16 [4096], P('ra'), may hold values from 0.099609375 to 1.8984375
Outputs:
- normed_out: bfloat16 [512, 4096], P('grp', 'ra'), parts along dimension 0
There are 2 independent parts, one for each index of `grp`. A program takes and returns all parts, laid end to end along the dimension named above; an argument that names none is the same for every part. Nothing has to cross between parts.
Inputs may be any that keep to these rules, and one draw needn't show every extreme that they name: `tokens`: feature scales differ along the width.
All inputs are finite; a program needn't handle non-finite values.
Results may differ from a plain program's by a relative error of at most 0.0059.
Values may be sent and summed in bfloat16 or wider, within the bound.
A program may use at most 64 MiB of HBM per device.

v0:
```python
import jax
import jax.numpy as jnp
from jax import lax
from jax.sharding import PartitionSpec as P

EPSILON = 1e-06
RESIDUAL_WEIGHT = 0.25


def spread(signal, kernel):
    padded = jnp.pad(signal, ((1, 1), (0, 0)))
    return padded[:-2] * kernel[0] + padded[1:-1] * kernel[1] + padded[2:] * kernel[2]


def activate(gate_sum, value_sum, kernel_gate, kernel_value, offset_gate, offset_value):
    gate_conv = spread(gate_sum, kernel_gate) + offset_gate
    value_conv = spread(value_sum, kernel_value) + offset_value
    return (jax.nn.silu(gate_conv) * value_conv).astype(jnp.bfloat16)


def body(
    tokens,
    norm_gain,
    w_gate,
    w_value,
    conv_gate,
    conv_value,
    bias_gate,
    bias_value,
    w_down,
    out_gain,
):
    wide_in = tokens.astype(jnp.float32)
    width = wide_in.shape[1] * lax.axis_size("ra")
    squares = lax.psum(jnp.sum(wide_in * wide_in, axis=1), "ra")
    rscale = lax.rsqrt(squares / width + EPSILON)
    normed = (wide_in * rscale[:, None] * norm_gain.astype(jnp.float32)).astype(jnp.bfloat16)
    part_gate = jnp.dot(normed, w_gate, preferred_element_type=jnp.float32)
    part_value = jnp.dot(normed, w_value, preferred_element_type=jnp.float32)
    gate_sum, value_sum = (
        lax.psum_scatter(part_gate, "ra", scatter_dimension=1, tiled=True),
        lax.psum_scatter(part_value, "ra", scatter_dimension=1, tiled=True),
    )
    share_cols = gate_sum.shape[1]
    first_col = lax.axis_index("ra") * share_cols
    local_hidden = activate(
        gate_sum,
        value_sum,
        lax.dynamic_slice_in_dim(conv_gate, first_col, share_cols, 1),
        lax.dynamic_slice_in_dim(conv_value, first_col, share_cols, 1),
        lax.dynamic_slice_in_dim(bias_gate, first_col, share_cols, 0),
        lax.dynamic_slice_in_dim(bias_value, first_col, share_cols, 0),
    )
    partial_value = jnp.dot(
        lax.all_gather(local_hidden, "ra", axis=1, tiled=True),
        w_down,
        preferred_element_type=jnp.float32,
    )
    branch = lax.psum(partial_value, "cb")
    summed = RESIDUAL_WEIGHT * wide_in + branch
    totals = lax.psum(jnp.sum(summed * summed, axis=1), "ra")
    oscale = lax.rsqrt(totals / width + EPSILON)
    return (summed * oscale[:, None] * out_gain.astype(jnp.float32)).astype(jnp.bfloat16)


def solution(mesh):
    return jax.shard_map(
        body,
        mesh=mesh,
        in_specs=(
            P("grp", "ra"),
            P("ra"),
            P("ra", "cb"),
            P("ra", "cb"),
            P(None, "cb"),
            P(None, "cb"),
            P("cb"),
            P("cb"),
            P("cb", "ra"),
            P("ra"),
        ),
        out_specs=P("grp", "ra"),
        check_vma=False,
    )
```

profile of v0, /device:TPU:0, one launch (start us, length us, event | category | flops | bytes accessed | tf_op | source)
XLA Modules:
  0.0 244.4 jit_solution(13220206293900376885)
XLA Ops:
  6.5 0.7 convert_element_type.22
  7.2 1.2 fusion.1
  8.4 13.5 %psum.21 = f32[256]{0:T(256)S(1)} all-reduce(f32[256]{0:T(256)S(1)} %fusion.1), channel_id=1, replica_groups=mesh['grp'=2,'ra'=4,'cb'=4] {'ra'}, use_global_device_ids=true, to_apply=%region_1.0 | all-reduce | flops 256 | bytes 2048 | tf_op jit(solution)/shard_map/psum | solution.py:35
  21.9 6.9 %fusion.16 = f32[256,2816]{0,1:T(8,128)} fusion(bf16[1024,2816]{1,0:T(8,128)(2,1)} %param.13, bf16[256,1024]{1,0:T(8,128)(2,1)} %param.10, f32[1024]{0:T(1024)S(1)} %convert_element_type.22, f32[256]{0:T(256)S(1)} %add_rsqrt_fusion.1), kind=kOutput, calls=%fused_computation.25 | convolution fusion | flops 1477443584 | bytes 9180160 | tf_op jit(solution)/shard_map/dot_general | solution.py:39
  28.8 0.0 reduce-scatter.5.cloned.1.call-update
  28.8 0.0 reduce-scatter.3.cloned.1.call-start
  28.9 6.7 %fusion.18 = f32[256,2816]{0,1:T(8,128)} fusion(bf16[1024,2816]{1,0:T(8,128)(2,1)} %param.12, bf16[256,1024]{1,0:T(8,128)(2,1)S(1)} %copy-done, f32[1024]{0:T(1024)S(1)} %convert_element_type.22, f32[256]{0:T(256)S(1)} %add_rsqrt_fusion.1), kind=kOutput, calls=%fused_computation.26 | convolution fusion | flops 1477443584 | bytes 9180160 | tf_op jit(solution)/shard_map/dot_general | solution.py:38
  35.5 0.0 reduce-scatter.3.cloned.1.call-update
  35.6 0.0 all-gather.2.cloned.1.call-start
  35.6 0.8 dynamic_slice.15
  36.4 0.8 dynamic_slice.13
  37.2 0.9 dynamic-slice_reduce_fusion.2
  38.1 45.4 %reduce-scatter.5.cloned.1.call-done = f32[256,704]{0,1:T(8,128)} async-done(((f32[256,2816]{0,1:T(8,128)}), f32[256,704]{0,1:T(8,128)}) %reduce-scatter.5.cloned.1.call-update) | async-done | bytes 720912 | tf_op jit(solution)/shard_map/reduce_scatter | solution.py:42
  83.5 58.4 %reduce-scatter.3.cloned.1.call-done = f32[256,704]{0,1:T(8,128)} async-done(((f32[256,2816]{0,1:T(8,128)}), f32[256,704]{0,1:T(8,128)}) %reduce-scatter.3.cloned.1.call-update) | async-done | bytes 720912 | tf_op jit(solution)/shard_map/reduce_scatter | solution.py:41
  141.9 4.6 %fusion.14 = bf16[256,704]{0,1:T(8,128)(2,1)} fusion(f32[256,704]{0,1:T(8,128)} %reduce-scatter.5.cloned.1.call-done, f32[256,704]{0,1:T(8,128)} %reduce-scatter.3.cloned.1.call-done, f32[704]{0:T(1024)S(1)} %dynamic_slice.15, f32[704]{0:T(1024)S(1)} %get-tuple-element.10, f32[704]{0:T(1024)S(1)} %get-tuple-element.9, f32[704]{0:T(1024)S(1)} %get-tuple-element.8, ...), kind=kLoop, calls=%fused_computation.23 | loop fusion | flops 3244032 | bytes 1824768 | tf_op jit(solution)/shard_map/convert_element_type | solution.py:18
  146.6 0.0 all-gather.2.cloned.1.call-update
  146.6 0.0 all-reduce.4.cloned.1.call-start
  146.6 34.6 %all-gather.2.cloned.1.call-done = bf16[256,2816]{0,1:T(8,128)(2,1)} async-done(((bf16[256,704]{0,1:T(8,128)(2,1)}), bf16[256,2816]{0,1:T(8,128)(2,1)}) %all-gather.2.cloned.1.call-update) | async-done | bytes 1441808 | tf_op jit(solution)/shard_map/all_gather | solution.py:55
  181.2 5.7 %fusion.20 = f32[256,1024]{1,0:T(8,128)} fusion(bf16[256,2816]{0,1:T(8,128)(2,1)} %all-gather.2.cloned.1.call-done, bf16[2816,1024]{1,0:T(8,128)(2,1)} %param.18), kind=kOutput, calls=%fused_computation.35 | convolution fusion | flops 1476395008 | bytes 8257536 | tf_op jit(solution)/shard_map/dot_general | solution.py:54
  187.0 0.0 all-reduce.4.cloned.1.call-update
  187.0 35.4 %all-reduce.4.cloned.1.call-done = f32[256,1024]{1,0:T(8,128)} async-done(((f32[256,1024]{1,0:T(8,128)}), f32[256,1024]{1,0:T(8,128)}) %all-reduce.4.cloned.1.call-update) | async-done | bytes 1048592 | tf_op jit(solution)/shard_map/psum | solution.py:59
  222.4 1.5 multiply_reduce_fusion
  223.9 11.7 %psum.23 = f32[256]{0:T(256)S(1)} all-reduce(f32[256]{0:T(256)S(1)} %multiply_reduce_fusion), channel_id=1, replica_groups=mesh['grp'=2,'ra'=4,'cb'=4] {'ra'}, use_global_device_ids=true, to_apply=%region_6.7 | all-reduce | flops 256 | bytes 2048 | tf_op jit(solution)/shard_map/psum | solution.py:61
  235.6 2.2 multiply_convert_fusion
  (8 shorter events, 0.0 us)
Async XLA Ops:
  6.5 77.0 %reduce-scatter.5.cloned.1.call-start = ((), (), s32[]{:S(2)}) async-start(), calls=%async_computation.3 | async-start | bytes 3604480 | tf_op jit(solution)/shard_map/reduce_scatter | solution.py:42
  21.9 6.9 %copy-start = (bf16[256,1024]{1,0:T(8,128)(2,1)S(1)}, bf16[256,1024]{1,0:T(8,128)(2,1)}, u32[]{:S(2)}) copy-start(bf16[256,1024]{1,0:T(8,128)(2,1)} %param.10) | copy-start | bytes 1572868
  28.8 113.1 %reduce-scatter.3.cloned.1.call-start = ((), (), s32[]{:S(2)}) async-start(), calls=%async_computation.2 | async-start | bytes 3604480 | tf_op jit(solution)/shard_map/reduce_scatter | solution.py:41
  35.6 145.7 %all-gather.2.cloned.1.call-start = ((), (), s32[]{:S(2)}) async-start(), calls=%async_computation.4 | async-start | bytes 1802240 | tf_op jit(solution)/shard_map/all_gather | solution.py:55
  146.6 40.4 %copy-start.1 = (bf16[1024]{0:T(1024)(128)(2,1)S(1)}, bf16[1024]{0:T(1024)(128)(2,1)}, u32[]{:S(2)}) copy-start(bf16[1024]{0:T(1024)(128)(2,1)} %param.19) | copy-start | bytes 6148
  146.6 75.8 %all-reduce.4.cloned.1.call-start = ((), (), s32[]{:S(2)}) async-start(), calls=%async_computation.5 | async-start | bytes 2097152 | tf_op jit(solution)/shard_map/psum | solution.py:59
Sparse Core Ops, SparseCore 0:
  28.9 54.5 reduce-scatter.4
  85.8 56.0 reduce-scatter.2
  146.7 34.4 all-gather.1
  187.1 35.2 all-reduce.3
where the time goes:
time: 245 us; the launch traced here: 244 us
  waiting for transfers between devices  174 us (71%)
  blocking collectives  25.2 us (10%)
  matrix products  19.3 us (8%)
  between operations  13.2 us (5%)
  other arithmetic  10.3 us (4%)
  local copies, waits for them, and re-layouts  2.5 us (1%)
    reduce_scatter x1, waiting for transfers between devices, body(): lax.psum_scatter(part_gate, 'ra', scatter_dimension=1, tiled=True)  58.4 us
    reduce_scatter x1, waiting for transfers between devices, body(): lax.psum_scatter(part_value, 'ra', scatter_dimension=1, tiled=True)  45.4 us
    psum x1, waiting for transfers between devices, body(): branch = lax.psum(partial_value, 'cb')  35.4 us
    all_gather x1, waiting for transfers between devices, body(): lax.all_gather(local_hidden, 'ra', axis=1, tiled=True)  34.6 us
    psum x1, blocking collectives, body(): squares = lax.psum(jnp.sum(wide_in * wide_in, axis=1), 'ra')  13.5 us
    psum x1, blocking collectives, body(): totals = lax.psum(jnp.sum(summed * summed, axis=1), 'ra')  11.7 us
    dot_general x1, matrix products, body(): part_value = jnp.dot(normed, w_value, preferred_element_type=jnp.float32)  6.85 us
    dot_general x1, matrix products, body(): part_gate = jnp.dot(normed, w_gate, preferred_element_type=jnp.float32)  6.67 us
  transfers between devices with their start and end apart: 4, of which 4 were waited for; matrix products, arithmetic and copies ran while one was open for 4% of the time, Pallas kernels for 0%

commit v1 on v0

--- a/solution.py
+++ b/solution.py
@@ -1,10 +1,18 @@
+import functools
+
 import jax
 import jax.numpy as jnp
 from jax import lax
+from jax.experimental import pallas as pl
+from jax.experimental.pallas import tpu as pltpu
 from jax.sharding import PartitionSpec as P
 
 EPSILON = 1e-06
 RESIDUAL_WEIGHT = 0.25
+MESH = pl.DeviceIdType.MESH
+LANES = 128
+SKEW = 2
+PIECES = 4
 
 
 def spread(signal, kernel):
@@ -18,7 +26,7 @@
     return (jax.nn.silu(gate_conv) * value_conv).astype(jnp.bfloat16)
 
 
-def body(
+def plain_body(
     tokens,
     norm_gain,
     w_gate,
@@ -63,7 +71,423 @@
     return (summed * oscale[:, None] * out_gain.astype(jnp.float32)).astype(jnp.bfloat16)
 
 
+def to_row(column):
+    rows = column.shape[0]
+    return jnp.transpose(jnp.broadcast_to(column, (rows, LANES)))[:8]
+
+
+def to_column(row):
+    return jnp.transpose(jnp.broadcast_to(row, (LANES, row.shape[1])))[:, :1]
+
+
+def shifted_sum(signal, taps, offset):
+    rows = signal.shape[0]
+    index = lax.broadcasted_iota(jnp.int32, signal.shape, 0)
+    before = jnp.where(index == 0, 0.0, pltpu.roll(signal, 1, 0))
+    after = jnp.where(index == rows - 1, 0.0, pltpu.roll(signal, rows - 1, 0))
+    return before * taps[0:1] + signal * taps[1:2] + after * taps[2:3] + offset
+
+
+def kernel(
+    ra_size,
+    tokens,
+    norm_gain,
+    w_gate,
+    w_value,
+    conv_gate,
+    conv_value,
+    bias_gate,
+    bias_value,
+    w_down,
+    out_gain,
+    out,
+    w_in,
+    w_out,
+    normed,
+    rs_out,
+    rs_in,
+    hid,
+    acc,
+    pair_in,
+    x_out,
+    x_in,
+    summed,
+    sq_col,
+    sq_first,
+    sq_last,
+    w_in_sem,
+    w_out_sem,
+    rs_send,
+    rs_recv,
+    hid_send,
+    hid_recv,
+    pair_send,
+    pair_recv,
+    x_send,
+    x_recv,
+    sum_send,
+    sum_recv,
+    first_send,
+    first_recv,
+    last_send,
+    last_recv,
+):
+    rows, wide = tokens.shape
+    chunks = hid.shape[0]
+    half = wide // 2
+    width = wide * ra_size
+    piece = rows // PIECES
+    last = ra_size - 1
+
+    me = lax.axis_index("ra")
+    cb = lax.axis_index("cb")
+    core = lax.rem(cb, 2)
+    partner = cb + 1 - 2 * core
+    across = lax.rem(cb + 2, 4)
+
+    place = (me, last - me)
+    ahead = (lax.rem(me + 1, ra_size), lax.rem(me + last, ra_size))
+    behind = (ahead[1], ahead[0])
+    lanes = (slice(LANES, 2 * LANES), slice(0, LANES))
+
+    def w_in_copies(chunk):
+        cols = pl.ds(pl.multiple_of(chunk * LANES, LANES), LANES)
+        return [
+            pltpu.make_async_copy(
+                w.at[:, cols], w_in.at[chunk, :, n * LANES : (n + 1) * LANES], w_in_sem.at[n, chunk]
+            )
+            for n, w in enumerate((w_gate, w_value))
+        ]
+
+    def w_out_copies(k):
+        return [
+            pltpu.make_async_copy(
+                w_down.at[pl.ds(pl.multiple_of((k + n * chunks) * LANES, LANES), LANES), :],
+                w_out.at[k, n * LANES : (n + 1) * LANES, :],
+                w_out_sem.at[n, k],
+            )
+            for n in range(2)
+        ]
+
+    def rs_copy(d, k):
+        return pltpu.make_async_remote_copy(
+            src_ref=rs_out.at[d, k],
+            dst_ref=rs_in.at[d, k],
+            send_sem=rs_send.at[d, k],
+            recv_sem=rs_recv.at[d, k],
+            device_id={"ra": ahead[d]},
+            device_id_type=MESH,
+        )
+
+    def hid_copy(d, k):
+        return pltpu.make_async_remote_copy(
+            src_ref=hid.at[k, :, lanes[d]],
+            dst_ref=hid.at[k, :, lanes[d]],
+            send_sem=hid_send.at[d, k],
+            recv_sem=hid_recv.at[d, k],
+            device_id={"ra": behind[d]},
+            device_id_type=MESH,
+        )
+
+    barrier = pltpu.get_barrier_semaphore()
+    for step in range(1, ra_size):
+        for q in (cb, partner):
+            pl.semaphore_signal(
+                barrier, inc=1, device_id={"ra": lax.rem(me + step, ra_size), "cb": q}, device_id_type=MESH
+            )
+    for q in (partner, across):
+        pl.semaphore_signal(barrier, inc=1, device_id={"cb": q}, device_id_type=MESH)
+
+    @pl.loop(0, chunks)
+    def _(k):
+        for chunk in (k, k + chunks):
+            for copy in w_in_copies(chunk):
+                copy.start()
+
+    @pl.loop(0, chunks)
+    def _(k):
+        for copy in w_out_copies(k):
+            copy.start()
+
+    wide_in = tokens[...].astype(jnp.float32)
+    sq_first[me] = to_row(jnp.sum(wide_in * wide_in, axis=1, keepdims=True))
+    acc[...] = jnp.zeros_like(acc)
+    pl.semaphore_wait(barrier, 2 * last + 2)
+
+    def first_copy(step):
+        return pltpu.make_async_remote_copy(
+            src_ref=sq_first.at[me],
+            dst_ref=sq_first.at[me],
+            send_sem=first_send.at[step],
+            recv_sem=first_recv.at[me],
+            device_id={"ra": lax.rem(me + step, ra_size)},
+            device_id_type=MESH,
+        )
+
+    for step in range(1, ra_size):
+        first_copy(step).start()
+    for step in range(1, ra_size):
+        source = lax.rem(me + step, ra_size)
+        pltpu.make_async_remote_copy(
+            src_ref=sq_first.at[source],
+            dst_ref=sq_first.at[source],
+            send_sem=first_send.at[step],
+            recv_sem=first_recv.at[source],
+            device_id={"ra": source},
+            device_id_type=MESH,
+        ).wait_recv()
+    squares = sq_first[0, 0:1]
+    for n in range(1, ra_size):
+        squares = squares + sq_first[n, 0:1]
+    rscale = lax.rsqrt(to_column(squares) / width + EPSILON)
+    normed[...] = (tokens[...].astype(jnp.float32) * rscale * norm_gain[...].astype(jnp.float32)).astype(
+        jnp.bfloat16
+    )
+
+    def reduce_step(d, k):
+        chunk = k + chunks if d == 0 else k
+        for copy in w_in_copies(chunk):
+            copy.wait()
+        part = jnp.dot(normed[...], w_in[chunk], preferred_element_type=jnp.float32)
+
+        @pl.when(place[d] == 0)
+        def _():
+            rs_out[d, k] = part.astype(jnp.bfloat16)
+            rs_copy(d, k).start()
+
+        @pl.when(place[d] > 0)
+        def _():
+            rs_copy(d, k).wait_recv()
+            total = part + rs_in[d, k].astype(jnp.float32)
+
+            @pl.when(place[d] < last)
+            def _():
+                rs_out[d, k] = total.astype(jnp.bfloat16)
+                rs_copy(d, k).start()
+
+            @pl.when(place[d] == last)
+            def _():
+                cols = pl.ds(pl.multiple_of(chunk * LANES, LANES), LANES)
+                gate = shifted_sum(total[:, :LANES], conv_gate[:, cols], bias_gate[:, cols])
+                value = shifted_sum(total[:, LANES:], conv_value[:, cols], bias_value[:, cols])
+                hid[k, :, lanes[d]] = (gate / (1.0 + jnp.exp(-gate)) * value).astype(jnp.bfloat16)
+                hid_copy(d, k).start()
+
+    def down_step(k):
+        for copy in w_out_copies(k):
+            copy.wait()
+        for n in range(2):
+            acc[n] += jnp.dot(
+                hid[k], w_out[k, :, n * half : (n + 1) * half], preferred_element_type=jnp.float32
+            )
+
+    @pl.loop(0, chunks + 2 * SKEW * last)
+    def _(i):
+        for d in range(2):
+            k = i - SKEW * place[d]
+            pl.when((k >= 0) & (k < chunks))(functools.partial(reduce_step, d, k))
+        for d in range(2):
+            k = i - SKEW * (2 * last - place[d])
+
+            @pl.when((k >= 0) & (k < chunks) & (place[d] < last))
+            def _():
+                hid_copy(d, k).wait_recv()
+
+                @pl.when(place[d] > 0)
+                def _():
+                    hid_copy(d, k).start()
+
+        k = i - SKEW * (last + jnp.maximum(place[0], place[1]))
+        pl.when((k >= 0) & (k < chunks))(functools.partial(down_step, k))
+
+    def rows_of(p):
+        return pl.ds(p * piece, piece)
+
+    def pair_copy(p):
+        return pltpu.make_async_remote_copy(
+            src_ref=acc.at[1 - core, rows_of(p)],
+            dst_ref=pair_in.at[rows_of(p)],
+            send_sem=pair_send.at[p],
+            recv_sem=pair_recv.at[p],
+            device_id={"cb": partner},
+            device_id_type=MESH,
+        )
+
+    def x_copy(p):
+        return pltpu.make_async_remote_copy(
+            src_ref=x_out.at[rows_of(p)],
+            dst_ref=x_in.at[rows_of(p)],
+            send_sem=x_send.at[p],
+            recv_sem=x_recv.at[p],
+            device_id={"cb": across},
+            device_id_type=MESH,
+        )
+
+    def sum_copy(p, n):
+        return pltpu.make_async_remote_copy(
+            src_ref=summed.at[n, rows_of(p)],
+            dst_ref=summed.at[n, rows_of(p)],
+            send_sem=sum_send.at[p],
+            recv_sem=sum_recv.at[p],
+            device_id={"cb": partner},
+            device_id_type=MESH,
+        )
+
+    def last_copy(owner, n, ra, q):
+        return pltpu.make_async_remote_copy(
+            src_ref=sq_last.at[owner],
+            dst_ref=sq_last.at[owner],
+            send_sem=last_send.at[n],
+            recv_sem=last_recv.at[owner],
+            device_id={"ra": ra, "cb": q},
+            device_id_type=MESH,
+        )
+
+    for p in range(PIECES):
+        pair_copy(p).start()
+    for p in range(PIECES):
+        pair_copy(p).wait_recv()
+        x_out[rows_of(p), :] = (acc[core, rows_of(p)] + pair_in[rows_of(p), :]).astype(jnp.bfloat16)
+        x_copy(p).start()
+    own_cols = pl.ds(pl.multiple_of(core * half, LANES), half)
+    for p in range(PIECES):
+        x_copy(p).wait_recv()
+        branch = x_out[rows_of(p), :].astype(jnp.float32) + x_in[rows_of(p), :].astype(jnp.float32)
+        total = RESIDUAL_WEIGHT * tokens[rows_of(p), own_cols].astype(jnp.float32) + branch
+        summed[core, rows_of(p)] = total
+        sum_copy(p, core).start()
+        sq_col[rows_of(p), :] = jnp.broadcast_to(jnp.sum(total * total, axis=1, keepdims=True), (piece, LANES))
+
+    mine = 2 * me + core
+    sq_last[mine] = jnp.transpose(sq_col[...])[:8]
+    targets = [(me, partner)]
+    for step in range(1, ra_size):
+        targets += [(lax.rem(me + step, ra_size), q) for q in (cb, partner)]
+    for n, (ra, q) in enumerate(targets):
+        last_copy(mine, n, ra, q).start()
+    for p in range(PIECES):
+        sum_copy(p, 1 - core).wait_recv()
+    for n, (ra, q) in enumerate(targets):
+        last_copy(2 * ra + lax.rem(q, 2), n, ra, q).wait_recv()
+    totals = sq_last[0, 0:1]
+    for n in range(1, 2 * ra_size):
+        totals = totals + sq_last[n, 0:1]
+    oscale = lax.rsqrt(to_column(totals) / width + EPSILON)
+    for n in range(2):
+        cols = slice(n * half, (n + 1) * half)
+        out[:, cols] = (summed[n] * oscale * out_gain[:, cols].astype(jnp.float32)).astype(jnp.bfloat16)
+
+    for step in range(1, ra_size):
+        first_copy(step).wait_send()
+    for d in range(2):
+
+        @pl.loop(0, chunks)
+        def _(k):
+            @pl.when(place[d] < last)
+            def _():
+                rs_copy(d, k).wait_send()
+
+            @pl.when(place[d] > 0)
+            def _():
+                hid_copy(d, k).wait_send()
+
+    for p in range(PIECES):
+        pair_copy(p).wait_send()
+        x_copy(p).wait_send()
+        sum_copy(p, core).wait_send()
+    for n, (ra, q) in enumerate(targets):
+        last_copy(mine, n, ra, q).wait_send()
+
+
+def fused_body(
+    tokens,
+    norm_gain,
+    w_gate,
+    w_value,
+    conv_gate,
+    conv_value,
+    bias_gate,
+    bias_value,
+    w_down,
+    out_gain,
+):
+    ra_size = lax.axis_size("ra")
+    rows, wide = tokens.shape
+    chunks = w_gate.shape[1] // (2 * LANES)
+    vmem = pl.BlockSpec(memory_space=pltpu.VMEM)
+    anywhere = pl.BlockSpec(memory_space=pl.ANY)
+    f32, bf16 = jnp.float32, jnp.bfloat16
+    dma = pltpu.SemaphoreType.DMA
+    return pl.pallas_call(
+        functools.partial(kernel, ra_size),
+        out_shape=jax.ShapeDtypeStruct((rows, wide), bf16),
+        in_specs=[vmem, vmem, anywhere, anywhere, vmem, vmem, vmem, vmem, anywhere, vmem],
+        out_specs=vmem,
+        scratch_shapes=[
+            pltpu.VMEM((2 * chunks, wide, 2 * LANES), bf16),
+            pltpu.VMEM((chunks, 2 * LANES, wide), bf16),
+            pltpu.VMEM((rows, wide), bf16),
+            pltpu.VMEM((2, chunks, rows, 2 * LANES), bf16),
+            pltpu.VMEM((2, chunks, rows, 2 * LANES), bf16),
+            pltpu.VMEM((chunks, rows, 2 * LANES), bf16),
+            pltpu.VMEM((2, rows, wide // 2), f32),
+            pltpu.VMEM((rows, wide // 2), f32),
+            pltpu.VMEM((rows, wide // 2), bf16),
+            pltpu.VMEM((rows, wide // 2), bf16),
+            pltpu.VMEM((2, rows, wide // 2), f32),
+            pltpu.VMEM((rows, LANES), f32),
+            pltpu.VMEM((ra_size, 8, rows), f32),
+            pltpu.VMEM((2 * ra_size, 8, rows), f32),
+            dma((2, 2 * chunks)),
+            dma((2, chunks)),
+            dma((2, chunks)),
+            dma((2, chunks)),
+            dma((2, chunks)),
+            dma((2, chunks)),
+            dma((PIECES,)),
+            dma((PIECES,)),
+            dma((PIECES,)),
+            dma((PIECES,)),
+            dma((PIECES,)),
+            dma((PIECES,)),
+            dma((ra_size,)),
+            dma((ra_size,)),
+            dma((2 * ra_size,)),
+            dma((2 * ra_size,)),
+        ],
+        compiler_params=pltpu.CompilerParams(
+            collective_id=0, has_side_effects=True, vmem_limit_bytes=56 * 1024 * 1024
+        ),
+    )(
+        tokens,
+        norm_gain.reshape(1, -1),
+        w_gate,
+        w_value,
+        conv_gate,
+        conv_value,
+        bias_gate.reshape(1, -1),
+        bias_value.reshape(1, -1),
+        w_down,
+        out_gain.reshape(1, -1),
+    )
+
+
 def solution(mesh):
+    ra_size, cb_size = mesh.shape["ra"], mesh.shape["cb"]
+
+    def body(*args):
+        rows, wide = args[0].shape
+        hidden = args[2].shape[1]
+        fits = (
+            ra_size >= 2
+            and cb_size == 4
+            and rows % LANES == 0
+            and wide % (2 * LANES) == 0
+            and hidden % (2 * LANES) == 0
+            and 3 * 2 * wide * hidden + 10 * rows * hidden + 20 * rows * wide < 48 * 1024 * 1024
+        )
+        return fused_body(*args) if fits else plain_body(*args)
+
     return jax.shard_map(
         body,
         mesh=mesh,

time: 245 us -> 94.8 us (0.39)
  waiting for transfers between devices: 174 us -> 0 us
  Pallas kernels: 0 us -> 87.4 us
  blocking collectives: 25.2 us -> 0 us
  matrix products: 19.3 us -> 0 us
  between operations: 13.2 us -> 0.01 us
  other arithmetic: 10.3 us -> 0 us
  local copies, waits for them, and re-layouts: 2.5 us -> 7.04 us
    reduce_scatter x2 -> x0, waiting for transfers between devices: 104 us -> none  [the longest x1 58.4 us: body(): lax.psum_scatter(part_gate, 'ra', scatter_dimension=1, tiled=True)]
    pallas_call x0 -> x1, Pallas kernels: none -> 87.4 us  [fused_body(): pl.pallas_call(functools.partial(kernel, ra_size), out_shape=jax.ShapeDty...]
    psum x1 -> x0, waiting for transfers between devices: 35.4 us -> none  [body(): branch = lax.psum(partial_value, 'cb')]
    all_gather x1 -> x0, waiting for transfers between devices: 34.6 us -> none  [body(): lax.all_gather(local_hidden, 'ra', axis=1, tiled=True)]
    psum x2 -> x0, blocking collectives: 25.2 us -> none  [the longest x1 13.5 us: body(): squares = lax.psum(jnp.sum(wide_in * wide_in, axis=1), 'ra')]
    dot_general x3 -> x0, matrix products: 19.3 us -> none  [the longest x1 6.85 us: body(): part_value = jnp.dot(normed, w_value, preferred_element_type=jnp.float32)]
    convert_element_type x4 -> x0, other arithmetic: 7.55 us -> none  [the longest x1 4.64 us: activate(): return (jax.nn.silu(gate_conv) * value_conv).astype(jnp.bfloat16)]
    reshape x0 -> x4, local copies, waits for them, and re-layouts: none -> 5.17 us  [the longest x1 1.31 us: fused_body(): bias_gate.reshape(1, -1)]
  transfers between devices with their start and end apart: 4 -> 0, of which waited for: 4 -> 0; matrix products, arithmetic and copies ran while one was open for 4% -> 0% of each run, Pallas kernels for 0% -> 0%
where the time goes in v1:
time: 94.8 us; the launch traced here: 94.5 us
  Pallas kernels  87.4 us (92%)
  local copies, waits for them, and re-layouts  7.04 us (7%)
    pallas_call x1, Pallas kernels, fused_body(): pl.pallas_call(functools.partial(kernel, ra_size), out_shape=jax.ShapeDty...  87.4 us

profile of v1, /device:TPU:0, one launch (start us, length us, event | category | flops | bytes accessed | tf_op | source)
XLA Modules:
  0.0 94.5 jit_solution(7469079071375458297)
XLA Ops:
  0.0 1.3 %reshape.12.norm_gain = bf16[1,1024]{1,0:T(2,128)(2,1)} reshape(bf16[1024]{0:T(1024)(128)(2,1)} %param.11) | data formatting | bytes 4096 | tf_op jit(solution)/shard_map/reshape | solution.py:463
  1.3 1.3 %reshape.15.out_gain = bf16[1,1024]{1,0:T(2,128)(2,1)} reshape(bf16[1024]{0:T(1024)(128)(2,1)} %param.19) | data formatting | bytes 4096 | tf_op jit(solution)/shard_map/reshape | solution.py:471
  2.5 1.3 %reshape.13.bias_gate = f32[1,2816]{1,0:T(1,128)} reshape(f32[2816]{0:T(1024)} %param.16) | data formatting | bytes 22528 | tf_op jit(solution)/shard_map/reshape | solution.py:468
  3.9 1.3 %reshape.14.bias_value = f32[1,2816]{1,0:T(1,128)} reshape(f32[2816]{0:T(1024)} %param.17) | data formatting | bytes 22528 | tf_op jit(solution)/shard_map/reshape | solution.py:469
  5.2 87.4 %shard_map.100 = bf16[256,1024]{1,0:T(8,128)(2,1)} custom-call(bf16[256,1024]{1,0:T(8,128)(2,1)} %tokens.1, bf16[1,1024]{1,0:T(2,128)(2,1)} %reshape.12.norm_gain, bf16[1024,2816]{1,0:T(8,128)(2,1)} %w_gate.1, bf16[1024,2816]{1,0:T(8,128)(2,1)} %w_value.1, f32[3,2816]{1,0:T(4,128)} %conv_gate.1, f32[3,2816]{1,0:T(4,128)} %conv_value.1, ...), custom_call_target="tpu_custom_call" | custom-call | tf_op jit(solution)/shard_map/pallas_call | solution.py:421
  92.6 1.9 %copy.12 = bf16[256,1024]{1,0:T(8,128)(2,1)} copy(bf16[256,1024]{1,0:T(8,128)(2,1)} %shard_map.100) | data formatting | bytes 1048576

commit v2 on v1

--- a/solution.py
+++ b/solution.py
@@ -11,8 +11,12 @@
 RESIDUAL_WEIGHT = 0.25
 MESH = pl.DeviceIdType.MESH
 LANES = 128
+LEAD = 8
 SKEW = 2
+HOLD = 6
 PIECES = 4
+RS_CUTS = 2
+HID_CUTS = 1
 
 
 def spread(signal, kernel):
@@ -107,6 +111,7 @@
     rs_out,
     rs_in,
     hid,
+    part,
     acc,
     pair_in,
     x_out,
@@ -169,22 +174,25 @@
             for n in range(2)
         ]
 
-    def rs_copy(d, k):
-        return pltpu.make_async_remote_copy(
-            src_ref=rs_out.at[d, k],
-            dst_ref=rs_in.at[d, k],
-            send_sem=rs_send.at[d, k],
-            recv_sem=rs_recv.at[d, k],
+    def cut(c, cuts):
+        return slice(c * rows // cuts, (c + 1) * rows // cuts)
+
+    def rs_copy(d, k, c):
+        return pltpu.make_async_remote_copy(
+            src_ref=rs_out.at[d, k, cut(c, RS_CUTS)],
+            dst_ref=rs_in.at[d, k, cut(c, RS_CUTS)],
+            send_sem=rs_send.at[d, k, c],
+            recv_sem=rs_recv.at[d, k, c],
             device_id={"ra": ahead[d]},
             device_id_type=MESH,
         )
 
-    def hid_copy(d, k):
-        return pltpu.make_async_remote_copy(
-            src_ref=hid.at[k, :, lanes[d]],
-            dst_ref=hid.at[k, :, lanes[d]],
-            send_sem=hid_send.at[d, k],
-            recv_sem=hid_recv.at[d, k],
+    def hid_copy(d, k, c):
+        return pltpu.make_async_remote_copy(
+            src_ref=hid.at[k, cut(c, HID_CUTS), lanes[d]],
+            dst_ref=hid.at[k, cut(c, HID_CUTS), lanes[d]],
+            send_sem=hid_send.at[d, k, c],
+            recv_sem=hid_recv.at[d, k, c],
             device_id={"ra": behind[d]},
             device_id_type=MESH,
         )
@@ -240,7 +248,7 @@
     for n in range(1, ra_size):
         squares = squares + sq_first[n, 0:1]
     rscale = lax.rsqrt(to_column(squares) / width + EPSILON)
-    normed[...] = (tokens[...].astype(jnp.float32) * rscale * norm_gain[...].astype(jnp.float32)).astype(
+    normed[...] = (tokens[...].astype(jnp.float32) * rscale * norm_gain[...].astype(jnp.float32)[None, :]).astype(
         jnp.bfloat16
     )
 
@@ -248,30 +256,34 @@
         chunk = k + chunks if d == 0 else k
         for copy in w_in_copies(chunk):
             copy.wait()
-        part = jnp.dot(normed[...], w_in[chunk], preferred_element_type=jnp.float32)
+        part[d] = jnp.dot(normed[...], w_in[chunk], preferred_element_type=jnp.float32)
 
         @pl.when(place[d] == 0)
         def _():
-            rs_out[d, k] = part.astype(jnp.bfloat16)
-            rs_copy(d, k).start()
-
-        @pl.when(place[d] > 0)
+            for c in range(RS_CUTS):
+                at = cut(c, RS_CUTS)
+                rs_out[d, k, at] = part[d, at].astype(jnp.bfloat16)
+                rs_copy(d, k, c).start()
+
+        @pl.when((place[d] > 0) & (place[d] < last))
         def _():
-            rs_copy(d, k).wait_recv()
-            total = part + rs_in[d, k].astype(jnp.float32)
-
-            @pl.when(place[d] < last)
-            def _():
-                rs_out[d, k] = total.astype(jnp.bfloat16)
-                rs_copy(d, k).start()
-
-            @pl.when(place[d] == last)
-            def _():
-                cols = pl.ds(pl.multiple_of(chunk * LANES, LANES), LANES)
-                gate = shifted_sum(total[:, :LANES], conv_gate[:, cols], bias_gate[:, cols])
-                value = shifted_sum(total[:, LANES:], conv_value[:, cols], bias_value[:, cols])
-                hid[k, :, lanes[d]] = (gate / (1.0 + jnp.exp(-gate)) * value).astype(jnp.bfloat16)
-                hid_copy(d, k).start()
+            for c in range(RS_CUTS):
+                at = cut(c, RS_CUTS)
+                rs_copy(d, k, c).wait_recv()
+                rs_out[d, k, at] = (part[d, at] + rs_in[d, k, at].astype(jnp.float32)).astype(jnp.bfloat16)
+                rs_copy(d, k, c).start()
+
+        @pl.when(place[d] == last)
+        def _():
+            for c in range(RS_CUTS):
+                rs_copy(d, k, c).wait_recv()
+            total = part[d] + rs_in[d, k].astype(jnp.float32)
+            cols = pl.ds(pl.multiple_of(chunk * LANES, LANES), LANES)
+            gate = shifted_sum(total[:, :LANES], conv_gate[:, cols], bias_gate[cols][None, :])
+            value = shifted_sum(total[:, LANES:], conv_value[:, cols], bias_value[cols][None, :])
+            hid[k, :, lanes[d]] = (gate / (1.0 + jnp.exp(-gate)) * value).astype(jnp.bfloat16)
+            for c in range(HID_CUTS):
+                hid_copy(d, k, c).start()
 
     def down_step(k):
         for copy in w_out_copies(k):
@@ -281,23 +293,26 @@
                 hid[k], w_out[k, :, n * half : (n + 1) * half], preferred_element_type=jnp.float32
             )
 
-    @pl.loop(0, chunks + 2 * SKEW * last)
+    delay = LEAD + SKEW * (last - 1) + HOLD
+
+    @pl.loop(0, chunks + delay + SKEW * (last - 1))
     def _(i):
         for d in range(2):
-            k = i - SKEW * place[d]
+            k = i - jnp.where(place[d] == 0, 0, LEAD + SKEW * (place[d] - 1))
             pl.when((k >= 0) & (k < chunks))(functools.partial(reduce_step, d, k))
         for d in range(2):
-            k = i - SKEW * (2 * last - place[d])
+            k = i - delay - SKEW * (last - 1 - place[d])
 
             @pl.when((k >= 0) & (k < chunks) & (place[d] < last))
             def _():
-                hid_copy(d, k).wait_recv()
-
-                @pl.when(place[d] > 0)
-                def _():
-                    hid_copy(d, k).start()
-
-        k = i - SKEW * (last + jnp.maximum(place[0], place[1]))
+                for c in range(HID_CUTS):
+                    hid_copy(d, k, c).wait_recv()
+
+                    @pl.when(place[d] > 0)
+                    def _():
+                        hid_copy(d, k, c).start()
+
+        k = i - delay - SKEW * (jnp.maximum(place[0], place[1]) - 1)
         pl.when((k >= 0) & (k < chunks))(functools.partial(down_step, k))
 
     def rows_of(p):
@@ -375,7 +390,7 @@
     oscale = lax.rsqrt(to_column(totals) / width + EPSILON)
     for n in range(2):
         cols = slice(n * half, (n + 1) * half)
-        out[:, cols] = (summed[n] * oscale * out_gain[:, cols].astype(jnp.float32)).astype(jnp.bfloat16)
+        out[:, cols] = (summed[n] * oscale * out_gain[cols].astype(jnp.float32)[None, :]).astype(jnp.bfloat16)
 
     for step in range(1, ra_size):
         first_copy(step).wait_send()
@@ -385,11 +400,13 @@
         def _(k):
             @pl.when(place[d] < last)
             def _():
-                rs_copy(d, k).wait_send()
+                for c in range(RS_CUTS):
+                    rs_copy(d, k, c).wait_send()
 
             @pl.when(place[d] > 0)
             def _():
-                hid_copy(d, k).wait_send()
+                for c in range(HID_CUTS):
+                    hid_copy(d, k, c).wait_send()
 
     for p in range(PIECES):
         pair_copy(p).wait_send()
@@ -430,6 +447,7 @@
             pltpu.VMEM((2, chunks, rows, 2 * LANES), bf16),
             pltpu.VMEM((2, chunks, rows, 2 * LANES), bf16),
             pltpu.VMEM((chunks, rows, 2 * LANES), bf16),
+            pltpu.VMEM((2, rows, 2 * LANES), f32),
             pltpu.VMEM((2, rows, wide // 2), f32),
             pltpu.VMEM((rows, wide // 2), f32),
             pltpu.VMEM((rows, wide // 2), bf16),
@@ -440,10 +458,10 @@
             pltpu.VMEM((2 * ra_size, 8, rows), f32),
             dma((2, 2 * chunks)),
             dma((2, chunks)),
-            dma((2, chunks)),
-            dma((2, chunks)),
-            dma((2, chunks)),
-            dma((2, chunks)),
+            dma((2, chunks, RS_CUTS)),
+            dma((2, chunks, RS_CUTS)),
+            dma((2, chunks, HID_CUTS)),
+            dma((2, chunks, HID_CUTS)),
             dma((PIECES,)),
             dma((PIECES,)),
             dma((PIECES,)),
@@ -460,15 +478,15 @@
         ),
     )(
         tokens,
-        norm_gain.reshape(1, -1),
+        norm_gain,
         w_gate,
         w_value,
         conv_gate,
         conv_value,
-        bias_gate.reshape(1, -1),
-        bias_value.reshape(1, -1),
+        bias_gate,
+        bias_value,
         w_down,
-        out_gain.reshape(1, -1),
+        out_gain,
     )
 
 

time: 94.8 us -> 84.6 us (0.89)
  local copies, waits for them, and re-layouts: 7.04 us -> 1.87 us
  Pallas kernels: 87.4 us -> 82.5 us
    reshape x4 -> x0, local copies, waits for them, and re-layouts: 5.17 us -> none  [the longest x1 1.31 us: fused_body(): bias_gate.reshape(1, -1)]
    pallas_call x1, Pallas kernels: 87.4 us -> 82.5 us  [fused_body(): pl.pallas_call(functools.partial(kernel, ra_size), out_shape=jax.ShapeDty...]
where the time goes in v2:
time: 84.6 us; the launch traced here: 84.4 us
  Pallas kernels  82.5 us (98%)
  local copies, waits for them, and re-layouts  1.87 us (2%)
    pallas_call x1, Pallas kernels, fused_body(): pl.pallas_call(functools.partial(kernel, ra_size), out_shape=jax.ShapeDty...  82.5 us
    unnamed x1, local copies, waits for them, and re-layouts  1.87 us

profile of v2, /device:TPU:0, one launch (start us, length us, event | category | flops | bytes accessed | tf_op | source)
XLA Modules:
  0.0 84.4 jit_solution(8709373196904112890)
XLA Ops:
  0.0 82.5 %shard_map.100 = bf16[256,1024]{1,0:T(8,128)(2,1)} custom-call(bf16[256,1024]{1,0:T(8,128)(2,1)} %tokens.1, bf16[1024]{0:T(1024)(128)(2,1)} %norm_gain.1, bf16[1024,2816]{1,0:T(8,128)(2,1)} %w_gate.1, bf16[1024,2816]{1,0:T(8,128)(2,1)} %w_value.1, f32[3,2816]{1,0:T(4,128)} %conv_gate.1, f32[3,2816]{1,0:T(4,128)} %conv_value.1, f32[2816]{0:T(1024)} %bias_gate.1, ...), custom_call_target="tpu_custom_call" | custom-call | tf_op jit(solution)/shard_map/pallas_call | solution.py:438
  82.6 1.9 %copy.12 = bf16[256,1024]{1,0:T(8,128)(2,1)} copy(bf16[256,1024]{1,0:T(8,128)(2,1)} %shard_map.100) | data formatting | bytes 1048576
